TPU v7x, 512 devices: a 8x2x16 block of a 8x8x16 slice. The times are simulated.
512 devices in a mesh: grp: 2 (over y), dp: 8 (over x), kv: 16 (over z), tp: 2 (over core).
Axes of the slice: x: 8, y: 2, z: 16, core: 2. Of those that a mesh axis runs over, the one named last changes fastest.
The devices are a block of a 8x8x16 slice.
Arguments:
- tokens: bfloat16 [384, 4, 4096], P(('grp', 'dp'), None, ('kv', 'tp')), parts along dimension 0, may hold values from -6 to 6
- norm_gain: float32 [4096], replicated, may hold values from 0.1 to 1.9
- w_query: bfloat16 [16, 128, 4096], P('kv', 'tp'), may hold values from -0.09375 to 0.09375
- w_key: bfloat16 [16, 128, 4096], P('kv', 'tp'), may hold values from -0.09375 to 0.09375
- w_value: bfloat16 [16, 128, 4096], P('kv', 'tp'), may hold values from -0.09375 to 0.09375
- w_gate: bfloat16 [16, 128, 4096], P('kv', 'tp'), may hold values from -0.09375 to 0.09375
- w_decay: bfloat16 [4096, 16], replicated, may hold values from -0.09375 to 0.09375
- w_beta: bfloat16 [4096, 16], replicated, may hold values from -0.09375 to 0.09375
- decay_rate: float32 [16], P('kv'), may hold values from 0.02 to 1
- head_gain: float32 [128], P('tp'), may hold values from 0.1 to 1.9
- w_out: bfloat16 [16, 128, 4096], P('kv', 'tp'), may hold values from -0.1875 to 0.1875
- state: float32 [384, 16, 128, 128], P(('grp', 'dp'), 'kv', 'tp'), parts along dimension 0, may hold values from -6 to 6
- prev_keys: bfloat16 [384, 4, 16, 128], P(('grp', 'dp'), None, 'kv'), parts along dimension 0, may hold values from -6 to 6
- prev_values: bfloat16 [384, 4, 16, 128], P(('grp', 'dp'), None, 'kv', 'tp'), parts along dimension 0, may hold values from -6 to 6
- prev_decay: float32 [384, 4, 16], P(('grp', 'dp'), None, 'kv'), parts along dimension 0, may hold values from 0.01 to 1
- prev_beta: float32 [384, 4, 16], P(('grp', 'dp'), None, 'kv'), parts along dimension 0, may hold values from 0.05 to 1
- accepted: int32 [384], P(('grp', 'dp')), parts along dimension 0, may hold values from 0 to 4
Outputs:
- mixed: bfloat16 [384, 4, 4096], P(('grp', 'dp'), None, ('kv', 'tp')), parts along dimension 0
- committed: float32 [384, 16, 128, 128], P(('grp', 'dp'), 'kv', 'tp'), parts along dimension 0
There are 2 independent parts, one for each index of `grp`. A program takes and returns all parts, laid end to end along the dimension named above; an argument that names none is the same for every part. Nothing has to cross between parts.
All inputs are finite; a program needn't handle non-finite values.
Results may differ from a plain program's by a relative error of at most 0.015.
Values may be sent and summed in bfloat16 or wider, within the bound.
No kernel may reach another device: no remote copies, remote signals or barrier semaphores. Data moves between devices by JAX's collectives and lax.ppermute only.
A program may use at most 64 MiB of HBM per device.

v0:
```python
import jax
import jax.numpy as jnp
from jax import lax
from jax.sharding import PartitionSpec as P

DK = 128
DV = 128
EPS = 1e-06
PRECISE = lax.Precision.HIGHEST


def joined_along(parts, dim):
    parts = jnp.moveaxis(parts, 0, dim)
    shape = parts.shape
    return parts.reshape(*shape[:dim], shape[dim] * shape[dim + 1], *shape[dim + 2 :])


def gather_in_order(array, axes, sequence):
    parts = array[None]
    for k in sequence:
        parts = lax.all_gather(parts, axes[k], axis=0, tiled=True)
    current = [lax.axis_size(axes[k]) for k in reversed(sequence)]
    parts = parts.reshape(*current, *array.shape)
    turned = sorted(range(len(sequence)), key=lambda place: sequence[len(sequence) - 1 - place])
    return parts.transpose(*turned, *range(len(sequence), parts.ndim)).reshape(-1, *array.shape)


def gather_axes(array, axes, sequence, dim):
    return joined_along(gather_in_order(array, axes, sequence), dim)


def rows_first(arrays, axis, dims):
    turned = [jnp.moveaxis(a, dim, 0) for a, dim in zip(arrays, dims)]
    both = jnp.concatenate([t.reshape(len(t), -1) for t in turned], axis=1)
    out, at, finished = (lax.all_gather(both, axis, axis=0, tiled=True), 0, [])
    for t, dim in zip(turned, dims):
        share = out[:, at : at + t[0].size].reshape(-1, *t.shape[1:])
        finished.append(jnp.moveaxis(share, 0, dim))
        at += t[0].size
    return tuple(finished)


def total_of_pieces(array, axis):
    parts = lax.all_gather(array, axis)
    return parts.sum(axis=0)


def from_everyone(array, axis):
    copies = jnp.broadcast_to(array, (lax.axis_size(axis), *array.shape))
    return lax.all_to_all(copies, axis, split_axis=0, concat_axis=0, tiled=True)


def gathered_copies(array, axis, dim):
    parts = from_everyone(array, axis)
    return joined_along(parts, dim)


def from_partner(block, axis, bit):
    count = lax.axis_size(axis)
    route = []
    for low in range(count):
        high = low | 1 << bit
        if high != low and high < count:
            route += [(low, high), (high, low)]
    return lax.ppermute(block, axis, route)


def split_up(array, dim, devices):
    shape = array.shape
    parts = array.reshape(*shape[:dim], devices, shape[dim] // devices, *shape[dim + 1 :])
    return jnp.moveaxis(parts, dim, 0)


def sum_at_owner(array, axis, dim):
    parts = split_up(array, dim, lax.axis_size(axis))
    arrived = lax.all_to_all(parts, axis, split_axis=0, concat_axis=0, tiled=True)
    return arrived.astype(jnp.float32).sum(axis=0)


def unit_rows(values):
    return values * lax.rsqrt(jnp.sum(values * values, axis=-1, keepdims=True) + EPS)


def delta_update(carried, keys_now, values_now, retain, strength):
    carried = carried * retain[..., None, None]
    predicted = jnp.einsum("shed,shd->she", carried, keys_now, precision=PRECISE)
    update = strength[..., None] * (values_now - predicted)
    return carried + update[..., :, None] * keys_now[..., None, :]


def local(
    tokens,
    norm_gain,
    w_query,
    w_key,
    w_value,
    w_gate,
    w_decay,
    w_beta,
    decay_rate,
    head_gain,
    w_out,
    state,
    prev_keys,
    prev_values,
    prev_decay,
    prev_beta,
    accepted,
):
    gathered = gather_axes(tokens, ("kv", "tp"), (0, 1), 2)
    seq_local, proposals, width = gathered.shape
    row_count = seq_local * proposals
    floats = gathered.astype(jnp.float32)
    normed = (
        floats * lax.rsqrt(jnp.mean(floats * floats, axis=-1, keepdims=True) + EPS) * norm_gain
    ).astype(jnp.bfloat16)
    flat_rows = normed.reshape(row_count, width)
    heads_local = w_query.shape[0]

    def project(weight):
        product = lax.dot_general(
            flat_rows,
            weight.reshape(-1, width),
            (((1,), (1,)), ((), ())),
            preferred_element_type=jnp.float32,
        )
        return product.astype(jnp.bfloat16).reshape(seq_local, proposals, heads_local, -1)

    query_half = project(w_query)
    key_half = project(w_key)
    value_raw = project(w_value)
    gate_raw = project(w_gate)
    query_full, key_full = rows_first((query_half, key_half), "tp", (3, 3))
    head_start = lax.axis_index("kv") * heads_local
    decay_all = jnp.dot(flat_rows, w_decay, preferred_element_type=jnp.float32)
    beta_all = jnp.dot(flat_rows, w_beta, preferred_element_type=jnp.float32)
    decay_pre = lax.dynamic_slice_in_dim(decay_all, head_start, heads_local, 1).reshape(
        seq_local, proposals, heads_local
    )
    beta_pre = lax.dynamic_slice_in_dim(beta_all, head_start, heads_local, 1).reshape(
        seq_local, proposals, heads_local
    )
    forget = decay_rate * jax.nn.softplus(decay_pre)
    strength = jax.nn.sigmoid(beta_pre)
    queries = unit_rows(jax.nn.silu(query_full.astype(jnp.float32))) * DK ** (-0.5)
    key_unit = unit_rows(jax.nn.silu(key_full.astype(jnp.float32)))
    value_act = jax.nn.silu(value_raw.astype(jnp.float32))
    old_keys = unit_rows(prev_keys.astype(jnp.float32))
    old_values = prev_values.astype(jnp.float32)
    carried = state
    for position in range(proposals):
        accept_mask = (position < accepted).astype(jnp.float32)[:, None]
        carried = delta_update(
            carried,
            old_keys[:, position],
            old_values[:, position],
            jnp.exp(-prev_decay[:, position] * accept_mask),
            prev_beta[:, position] * accept_mask,
        )
    committed = carried
    outputs = []
    for position in range(proposals):
        carried = delta_update(
            carried,
            key_unit[:, position],
            value_act[:, position],
            jnp.exp(-forget[:, position]),
            strength[:, position],
        )
        outputs.append(
            jnp.einsum("shed,shd->she", carried, queries[:, position], precision=PRECISE)
        )
    heads_out = jnp.stack(outputs, axis=1)
    squares = total_of_pieces(jnp.sum(heads_out * heads_out, axis=-1), "tp")
    scaled = (
        heads_out
        * lax.rsqrt(squares[..., None] / DV + EPS)
        * head_gain
        * jax.nn.silu(gate_raw.astype(jnp.float32))
    ).astype(jnp.bfloat16)
    head_values = gathered_copies(scaled, "tp", 3)
    own_half = lax.axis_index("tp")
    kv_count = lax.axis_size("kv")
    col_block = w_out.shape[-1] // (kv_count * 2)
    grouped = w_out.reshape(heads_local, w_out.shape[1], kv_count, 2, col_block)
    own_rows = lax.dynamic_index_in_dim(grouped, own_half, 3, keepdims=False)
    other_rows = lax.dynamic_index_in_dim(grouped, 1 - own_half, 3, keepdims=False)
    received = from_partner(other_rows, "tp", 0)
    stacked = jnp.where(
        own_half == 0,
        jnp.concatenate([own_rows, received], axis=1),
        jnp.concatenate([received, own_rows], axis=1),
    )
    partial_value = jnp.dot(
        head_values.reshape(row_count, -1),
        stacked.reshape(-1, kv_count * col_block),
        preferred_element_type=jnp.float32,
    )
    mixed_out = sum_at_owner(partial_value.astype(jnp.bfloat16), "kv", 1)
    return (mixed_out.astype(jnp.bfloat16).reshape(seq_local, proposals, -1), committed)


def solution(mesh):
    in_specs = (
        P(("grp", "dp"), None, ("kv", "tp")),
        P(),
        P("kv", "tp", None),
        P("kv", "tp", None),
        P("kv", "tp", None),
        P("kv", "tp", None),
        P(),
        P(),
        P("kv"),
        P("tp"),
        P("kv", "tp", None),
        P(("grp", "dp"), "kv", "tp", None),
        P(("grp", "dp"), None, "kv", None),
        P(("grp", "dp"), None, "kv", "tp"),
        P(("grp", "dp"), None, "kv"),
        P(("grp", "dp"), None, "kv"),
        P(("grp", "dp")),
    )
    out_specs = (P(("grp", "dp"), None, ("kv", "tp")), P(("grp", "dp"), "kv", "tp", None))
    return jax.shard_map(local, mesh=mesh, in_specs=in_specs, out_specs=out_specs, check_vma=False)
```

profile of v0, /device:TPU:92, one launch (start us, length us, event | category | flops | bytes accessed | tf_op | source)
XLA Modules:
  0.0 155.5 jit_solution(11269415672865246315)
XLA Ops:
  0.7 1.5 reshape.799
  2.1 2.1 %dynamic-slice_reduce_fusion = (bf16[64,16,128]{2,1,0:T(8,128)(2,1)S(1)}, bf16[1,64,16,1,128]{4,3,2,1,0:T(2,128)(2,1)S(1)}) fusion(bf16[1,64,16,2,128]{4,3,2,1,0:T(2,128)(2,1)S(1)} %reshape.799, s32[]{:T(128)S(6)} %select_n.37, s32[]{:T(128)S(6)} %select_n.38), kind=kLoop, calls=%fused_computation.67 | loop fusion | bytes 1048584 | tf_op jit(solution)/shard_map/jit(dynamic_index_in_dim)/dynamic_slice | solution.py:186
  4.3 2.0 %collective-permute-start = (bf16[1,64,16,128]{3,2,1,0:T(8,128)(2,1)S(1)}, bf16[1,64,16,128]{3,2,1,0:T(8,128)(2,1)}, u32[]{:S(2)}, u32[]{:S(2)}) collective-permute-start(bf16[1,64,16,128]{3,2,1,0:T(8,128)(2,1)S(1)} %bitcast.318), channel_id=1, source_target_pairs={{0,1},{1,0},{2,3},{3,2},{4,5},{5,4},{6,7},{7,6},{8,9},{9,8},{10,11... | collective-permute-start | bytes 786440 | tf_op jit(solution)/shard_map/ppermute | solution.py:65
  8.4 70.1 %all-gather = bf16[384,4,128]{2,0,1:T(8,128)(2,1)S(1)} all-gather(bf16[24,4,128]{2,0,1:T(8,128)(2,1)S(1)} %copy.110), channel_id=2, replica_groups=mesh['grp'=2,'dp'=8,'kv'=16,'tp'=2] {'kv'}, dimensions={0}, use_global_device_ids=true | all-gather | bytes 417792 | tf_op jit(solution)/shard_map/all_gather | solution.py:21
  78.5 2.4 %all_gather.16 = bf16[32,24,4,128]{3,1,0,2:T(8,128)(2,1)S(1)} all-gather(bf16[16,24,4,128]{3,1,0,2:T(8,128)(2,1)S(1)} %bitcast.308), channel_id=1, replica_groups=mesh['grp'=2,'dp'=8,'kv'=16,'tp'=2] {'tp'}, dimensions={0}, use_global_device_ids=true | all-gather | bytes 1179648 | tf_op jit(solution)/shard_map/all_gather | solution.py:21
  83.3 1.5 convolution_convert_fusion.3
  85.0 2.1 %all_gather.17 = bf16[128,192]{1,0:T(8,128)(2,1)S(1)} all-gather(bf16[64,192]{1,0:T(8,128)(2,1)S(1)} %copy.119), channel_id=1, replica_groups=mesh['grp'=2,'dp'=8,'kv'=16,'tp'=2] {'tp'}, dimensions={0}, use_global_device_ids=true | all-gather | bytes 73728 | tf_op jit(solution)/shard_map/all_gather | solution.py:35
  87.1 1.5 fusion.3
  88.6 2.1 %fusion.4 = f32[96,64]{0,1:T(8,128)} fusion(bf16[1,64,4096]{2,1,0:T(8,128)(2,1)} %param.21, bf16[12,8,32,128]{3,2,1,0:T(8,128)(2,1)S(1)} %bitcast.313), kind=kOutput, calls=%fused_computation.12 | convolution fusion | flops 50343936 | bytes 1335296 | tf_op jit(solution)/shard_map/dot_general | solution.py:121
  96.2 1.4 fusion.32
  97.7 1.5 fusion.30
  99.3 1.7 %fusion.28 = f32[24,1,64]{2,1,0:T(1,128)S(1)} fusion(f32[24]{0:T(128)S(1)} %get-tuple-element.38, f32[24,128]{1,0:T(8,128)S(1)} %bitcast.333, f32[24,64]{1,0:T(8,128)S(1)} %subtract_multiply_fusion.6, f32[24,4,1,128]{3,1,2,0:T(4,128)S(1)} %convert_multiply_fusion, f32[24,1,64,128]{3,2,1,0:T(8,128)S(1)} %copy-done.1, f32[24]{0:T(128)S(1)} %get-tuple-element.40, ...), kind=kOutput, calls=%fused_computation.36 | convolution fusion | flops 3735552 | bytes 855552 | tf_op jit(solution)/shard_map/shed,shd->she/dot_general | solution.py:86
  101.1 2.3 %fusion.26 = f32[24,1,64]{2,1,0:T(1,128)S(1)} fusion(f32[24]{0:T(128)S(1)} %get-tuple-element.39, f32[24,128]{1,0:T(8,128)S(1)} %bitcast.330, f32[24,64]{1,0:T(8,128)S(1)} %subtract_multiply_fusion.5, f32[24]{0:T(128)S(1)} %get-tuple-element.38, f32[24,128]{1,0:T(8,128)S(1)} %bitcast.334, f32[24,64]{1,0:T(8,128)S(1)} %subtract_multiply_fusion.6, ...), kind=kOutput, calls=%fused_computation.34 | convolution fusion | flops 4325376 | bytes 880640 | tf_op jit(solution)/shard_map/shed,shd->she/dot_general | solution.py:86
  104.7 1.4 fusion.24
  106.1 1.4 fusion.22
  107.6 1.5 fusion.20
  109.1 1.8 %multiply_add_fusion.1 = f32[24,1,64,128]{3,2,1,0:T(8,128)S(1)} fusion(f32[24,128]{1,0:T(8,128)S(1)} %bitcast.349, f32[24,64]{1,0:T(8,128)S(1)} %subtract_multiply_fusion.2, f32[24]{0:T(128)S(1)} %get-tuple-element.8, f32[24,128]{1,0:T(8,128)S(1)} %bitcast.339, f32[24,64]{1,0:T(8,128)S(1)} %subtract_multiply_fusion.3, f32[24]{0:T(128)S(1)} %get-tuple-element.9, ...), kind=kLoop, calls=%fused_computation.45 | loop fusion | flops 3538944 | bytes 1684032 | tf_op jit(solution)/shard_map/add | solution.py:88
  112.2 1.4 fusion.16
  113.7 1.4 fusion.14
  115.1 1.5 fusion.12
  116.7 1.7 %fusion.10 = f32[24,1,64]{2,1,0:T(1,128)S(1)} fusion(f32[24,1,64,128]{3,2,1,0:T(8,128)S(1)} %multiply_add_fusion.1, f32[24,128]{1,0:T(8,128)S(1)} %bitcast.367, f32[24,64]{1,0:T(8,128)S(1)} %subtract_multiply_fusion, f32[24]{0:T(128)S(1)} %get-tuple-element.7, f32[24,128]{1,0:T(8,128)S(1)} %bitcast.360, f32[24,64]{1,0:T(8,128)S(1)} %subtract_multiply_fusion.1, ...), kind=kOutput, calls=%fused_computation.18 | convolution fusion | flops 3538944 | bytes 855040 | tf_op jit(solution)/shard_map/shed,shd->she/dot_general | solution.py:171
  118.4 1.9 %all-gather.2 = f32[2,24,4]{1,2,0:T(4,128)S(1)} all-gather(f32[1,24,4]{1,2,0:T(4,128)S(1)} %bitcast.373), channel_id=3, replica_groups=mesh['grp'=2,'dp'=8,'kv'=16,'tp'=2] {'tp'}, dimensions={0}, use_global_device_ids=true | all-gather | bytes 1152 | tf_op jit(solution)/shard_map/all_gather | solution.py:44
  121.2 3.3 %all-to-all-start = ((bf16[2,2,3072]{2,1,0:T(2,128)(2,1)}), bf16[2,2,3072]{2,1,0:T(2,128)(2,1)S(1)}, u32[]{:S(2)}, u32[]{:S(2)}) async-start(bf16[2,2,3072]{2,1,0:T(2,128)(2,1)} %reshape.862), calls=%async_computation | async-start | bytes 49152 | tf_op jit(solution)/shard_map/all_to_all | solution.py:50
  127.5 27.3 %all_to_all.10 = bf16[16,96,128]{2,1,0:T(8,128)(2,1)S(1)} all-to-all(bf16[16,96,128]{2,1,0:T(8,128)(2,1)S(1)} %bitcast.307), channel_id=1, replica_groups=mesh['grp'=2,'dp'=8,'kv'=16,'tp'=2] {'kv'}, dimensions={0} | all-to-all | bytes 786432 | tf_op jit(solution)/shard_map/all_to_all | solution.py:76
  (119 shorter events, 17.1 us)
Async XLA Ops:
  0.6 82.2 %copy-start = (bf16[1,64,4096]{2,1,0:T(8,128)(2,1)S(1)}, bf16[1,64,4096]{2,1,0:T(8,128)(2,1)}, u32[]{:S(2)}) copy-start(bf16[1,64,4096]{2,1,0:T(8,128)(2,1)} %param.20) | copy-start | bytes 1572868
  2.1 4.8 %copy-start.10 = (bf16[24,4,1,128]{3,1,2,0:T(4,128)(2,1)S(1)}, bf16[24,4,1,128]{3,1,2,0:T(4,128)(2,1)}, u32[]{:S(2)}) copy-start(bf16[24,4,1,128]{3,1,2,0:T(4,128)(2,1)} %param.29) | copy-start | bytes 73732
  2.1 4.9 %copy-start.17 = (bf16[24,4,128]{2,1,0:T(4,128)(2,1)S(1)}, bf16[24,4,128]{2,1,0:T(4,128)(2,1)}, u32[]{:S(2)}) copy-start(bf16[24,4,128]{2,1,0:T(4,128)(2,1)} %param.17) | copy-start | bytes 73732
  2.1 5.7 %copy-start.9 = (bf16[24,4,1,64]{3,1,2,0:T(4,128)(2,1)S(1)}, bf16[24,4,1,64]{3,1,2,0:T(4,128)(2,1)}, u32[]{:S(2)}) copy-start(bf16[24,4,1,64]{3,1,2,0:T(4,128)(2,1)} %param.30) | copy-start | bytes 36868
  4.3 121.8 %collective-permute-start = (bf16[1,64,16,128]{3,2,1,0:T(8,128)(2,1)S(1)}, bf16[1,64,16,128]{3,2,1,0:T(8,128)(2,1)}, u32[]{:S(2)}, u32[]{:S(2)}) collective-permute-start(bf16[1,64,16,128]{3,2,1,0:T(8,128)(2,1)S(1)} %bitcast.318), channel_id=1, source_target_pairs={{0,1},{1,0},{2,3},{3,2},{4,5},{5,4},{6,7},{7,6},{8,9},{9,8},{10,11... | collective-permute-start | bytes 786440 | tf_op jit(solution)/shard_map/ppermute | solution.py:65
  81.2 1.0 copy-start.11
  92.5 1.0 copy-start.12
  93.4 1.3 copy-start.3
  93.5 1.7 %copy-start.4 = (bf16[4096,16]{0,1:T(8,128)(2,1)S(1)}, bf16[4096,16]{0,1:T(8,128)(2,1)}, u32[]{:S(2)}) copy-start(bf16[4096,16]{0,1:T(8,128)(2,1)} %param.23) | copy-start | bytes 393220
  94.7 1.4 copy-start.18
  94.7 1.4 copy-start.19
  94.8 1.4 copy-start.22
  94.8 1.5 copy-start.1
  94.8 2.9 %copy-start.16 = (f32[24,1,1,64]{3,1,2,0:T(1,128)S(1)}, f32[24,1,1,64]{3,1,2,0:T(1,128)}, u32[]{:S(2)}) copy-start(f32[24,1,1,64]{3,1,2,0:T(1,128)} %get-tuple-element.26) | copy-start | bytes 18436
  94.8 2.9 %copy-start.5 = (f32[24,1,1,128]{3,1,2,0:T(1,128)S(1)}, f32[24,1,1,128]{3,1,2,0:T(1,128)}, u32[]{:S(2)}) copy-start(f32[24,1,1,128]{3,1,2,0:T(1,128)} %get-tuple-element.22) | copy-start | bytes 36868
  95.1 4.1 %copy-start.15 = (f32[24,1,1,64]{3,1,2,0:T(1,128)S(1)}, f32[24,1,1,64]{3,1,2,0:T(1,128)}, u32[]{:S(2)}) copy-start(f32[24,1,1,64]{3,1,2,0:T(1,128)} %get-tuple-element.27) | copy-start | bytes 18436
  95.1 4.2 %copy-start.8 = (f32[24,1,1,128]{3,1,2,0:T(1,128)S(1)}, f32[24,1,1,128]{3,1,2,0:T(1,128)}, u32[]{:S(2)}) copy-start(f32[24,1,1,128]{3,1,2,0:T(1,128)} %get-tuple-element.25) | copy-start | bytes 36868
  97.6 3.3 %copy-start.14 = (f32[24,1,1,64]{3,1,2,0:T(1,128)S(1)}, f32[24,1,1,64]{3,1,2,0:T(1,128)}, u32[]{:S(2)}) copy-start(f32[24,1,1,64]{3,1,2,0:T(1,128)} %get-tuple-element.28) | copy-start | bytes 18436
  97.6 3.4 %copy-start.7 = (f32[24,1,1,128]{3,1,2,0:T(1,128)S(1)}, f32[24,1,1,128]{3,1,2,0:T(1,128)}, u32[]{:S(2)}) copy-start(f32[24,1,1,128]{3,1,2,0:T(1,128)} %get-tuple-element.24) | copy-start | bytes 36868
  101.0 2.4 %copy-start.13 = (f32[24,1,1,64]{3,1,2,0:T(1,128)S(1)}, f32[24,1,1,64]{3,1,2,0:T(1,128)}, u32[]{:S(2)}) copy-start(f32[24,1,1,64]{3,1,2,0:T(1,128)} %get-tuple-element.29) | copy-start | bytes 18436
  101.0 2.5 %copy-start.6 = (f32[24,1,1,128]{3,1,2,0:T(1,128)S(1)}, f32[24,1,1,128]{3,1,2,0:T(1,128)}, u32[]{:S(2)}) copy-start(f32[24,1,1,128]{3,1,2,0:T(1,128)} %get-tuple-element.23) | copy-start | bytes 36868
  104.6 6.2 %copy-start.2 = (f32[24,1,64,128]{3,2,1,0:T(8,128)}, f32[24,1,64,128]{3,2,1,0:T(8,128)S(1)}, u32[]{:S(2)}) copy-start(f32[24,1,64,128]{3,2,1,0:T(8,128)S(1)} %multiply_add_fusion.3) | copy-start | bytes 2359300
  115.1 5.2 %copy-start.21 = (f32[64]{0:T(128)S(1)}, f32[64]{0:T(128)}, u32[]{:S(2)}) copy-start(f32[64]{0:T(128)} %param.26) | copy-start | bytes 772
  121.2 4.6 %all-to-all-start = ((bf16[2,2,3072]{2,1,0:T(2,128)(2,1)}), bf16[2,2,3072]{2,1,0:T(2,128)(2,1)S(1)}, u32[]{:S(2)}, u32[]{:S(2)}) async-start(bf16[2,2,3072]{2,1,0:T(2,128)(2,1)} %reshape.862), calls=%async_computation | async-start | bytes 49152 | tf_op jit(solution)/shard_map/all_to_all | solution.py:50
  (1 other events, 1.0 us)
where the time goes:
time: 156 us
  blocking collectives  104 us (67%)
  matrix products  24.8 us (16%)
  local copies, waits for them, and re-layouts  11.2 us (7%)
  other arithmetic  7.28 us (5%)
  starting transfers between devices  5.23 us (3%)
  between operations  1.92 us (1%)
    all_gather x2, blocking collectives, gather_in_order(): parts = lax.all_gather(parts, axes[k], axis=0, tiled=True)  72.5 us
    all_to_all x1, blocking collectives, sum_at_owner(): lax.all_to_all(parts, axis, split_axis=0, concat_axis=0, tiled=True)  27.3 us
    dot_general x8, matrix products, delta_update(): jnp.einsum('shed,shd->she', carried, keys_now, precision=PRECISE)  12.6 us
    dot_general x4, matrix products, local(): jnp.einsum('shed,shd->she', carried, queries[:, position], precision=PREC...  5.88 us
    dot_general x4, matrix products, project(): lax.dot_general(flat_rows, weight.reshape(-1, width), (((1,), (1,)), ((),...  5.44 us
    all_to_all x1, starting transfers between devices, from_everyone(): return lax.all_to_all(copies, axis, split_axis=0, concat_axis=0, tiled=True)  3.28 us
  transfers between devices with their start and end apart: 2, of which 1 were waited for; matrix products, arithmetic and copies ran while one was open for 24% of the time, Pallas kernels for 0%

commit v1 on v0

--- a/solution.py
+++ b/solution.py
@@ -18,7 +18,10 @@
 def gather_in_order(array, axes, sequence):
     parts = array[None]
     for k in sequence:
-        parts = lax.all_gather(parts, axes[k], axis=0, tiled=True)
+        frame = axes[k]
+        parts = jnp.concatenate(
+            lax.all_to_all(jnp.stack([parts] * lax.axis_size(frame)), frame, 0, 0), axis=0
+        )
     current = [lax.axis_size(axes[k]) for k in reversed(sequence)]
     parts = parts.reshape(*current, *array.shape)
     turned = sorted(range(len(sequence)), key=lambda place: sequence[len(sequence) - 1 - place])

time: 156 us -> 142 us (0.910)
  the two profiles are of different devices: /device:TPU:92 before, /device:TPU:94 now
where the time goes in v1:
time: 142 us; the launch traced here: 141 us
  starting transfers between devices  45.6 us (32%)
  blocking collectives  42.1 us (30%)
  matrix products  24.8 us (17%)
  local copies, waits for them, and re-layouts  10.2 us (7%)
  other arithmetic  8.68 us (6%)
  waiting for transfers between devices  8.04 us (6%)
  between operations  1.97 us (1%)
    all_to_all x1, starting transfers between devices, gather_in_order(): lax.all_to_all(jnp.stack([parts] * lax.axis_size(frame)), frame, 0, 0)  43.7 us
    all_to_all x1, blocking collectives, sum_at_owner(): lax.all_to_all(parts, axis, split_axis=0, concat_axis=0, tiled=True)  30 us
    dot_general x8, matrix products, delta_update(): jnp.einsum('shed,shd->she', carried, keys_now, precision=PRECISE)  12.4 us
    all_to_all x1, waiting for transfers between devices, gather_in_order(): lax.all_to_all(jnp.stack([parts] * lax.axis_size(frame)), frame, 0, 0)  8.04 us
    dot_general x4, matrix products, local(): jnp.einsum('shed,shd->she', carried, queries[:, position], precision=PREC...  5.89 us
    dot_general x4, matrix products, project(): lax.dot_general(flat_rows, weight.reshape(-1, width), (((1,), (1,)), ((),...  5.55 us
    all_to_all x1, blocking collectives, gather_in_order(): lax.all_to_all(jnp.stack([parts] * lax.axis_size(frame)), frame, 0, 0)  4.38 us
    add x2, other arithmetic, delta_update(): return carried + update[..., :, None] * keys_now[..., None, :]  4.19 us
  transfers between devices with their start and end apart: 2, of which 1 were waited for; matrix products, arithmetic and copies ran while one was open for 9% of the time, Pallas kernels for 0%

profile of v1, /device:TPU:94, one launch (start us, length us, event | category | flops | bytes accessed | tf_op | source)
XLA Modules:
  0.0 141.5 jit_solution(12007246569175899592)
XLA Ops:
  2.3 43.7 %all-to-all-start = ((bf16[16,1,24,4,128]{4,2,3,1,0:T(8,128)(2,1)}), bf16[16,1,24,4,128]{4,2,3,1,0:T(8,128)(2,1)S(1)}, u32[]{:S(2)}, u32[]{:S(2)}) async-start(bf16[16,1,24,4,128]{4,2,3,1,0:T(8,128)(2,1)} %stack.31), calls=%async_computation | async-start | bytes 786432 | tf_op jit(solution)/shard_map/all_to_all | solution.py:23
  46.4 2.1 %dynamic-slice_reduce_fusion = (bf16[64,16,128]{2,1,0:T(8,128)(2,1)S(1)}, bf16[1,64,16,1,128]{4,3,2,1,0:T(2,128)(2,1)S(1)}) fusion(bf16[1,64,16,2,128]{4,3,2,1,0:T(2,128)(2,1)S(1)} %reshape.797, s32[]{:T(128)S(6)} %select_n.37, s32[]{:T(128)S(6)} %select_n.38), kind=kLoop, calls=%fused_computation.69 | loop fusion | bytes 1048584 | tf_op jit(solution)/shard_map/jit(dynamic_index_in_dim)/dynamic_slice | solution.py:189
  48.6 2.0 %collective-permute-start = (bf16[1,64,16,128]{3,2,1,0:T(8,128)(2,1)S(1)}, bf16[1,64,16,128]{3,2,1,0:T(8,128)(2,1)S(1)}, u32[]{:S(2)}, u32[]{:S(2)}) collective-permute-start(bf16[1,64,16,128]{3,2,1,0:T(8,128)(2,1)S(1)} %bitcast.316), channel_id=1, source_target_pairs={{0,1},{1,0},{2,3},{3,2},{4,5},{5,4},{6,7},{7,6},{8,9},{9,8},{10,11... | collective-permute-start | bytes 786440 | tf_op jit(solution)/shard_map/ppermute | solution.py:68
  52.4 1.5 %fusion.30 = f32[24,1,64]{2,1,0:T(1,128)S(1)} fusion(f32[24,4,1,128]{3,1,2,0:T(4,128)S(1)} %convert_multiply_fusion, f32[24,1,64,128]{3,2,1,0:T(8,128)S(1)} %copy-done.1, f32[24]{0:T(128)S(1)} %get-tuple-element.40, f32[24,128]{1,0:T(8,128)S(1)} %bitcast.322, f32[24,64]{1,0:T(8,128)S(1)} %subtract_multiply_fusion.7, f32[24]{0:T(128)S(1)} %get-tuple-element.41), kind=kOutput, calls=%fused_computation.39 | convolution fusion | flops 3145728 | bytes 830464 | tf_op jit(solution)/shard_map/shed,shd->she/dot_general | solution.py:89
  54.7 1.7 %fusion.28 = f32[24,1,64]{2,1,0:T(1,128)S(1)} fusion(f32[24]{0:T(128)S(1)} %get-tuple-element.38, f32[24,128]{1,0:T(8,128)S(1)} %bitcast.332, f32[24,64]{1,0:T(8,128)S(1)} %subtract_multiply_fusion.6, f32[24,4,1,128]{3,1,2,0:T(4,128)S(1)} %convert_multiply_fusion, f32[24,1,64,128]{3,2,1,0:T(8,128)S(1)} %copy-done.1, f32[24]{0:T(128)S(1)} %get-tuple-element.40, ...), kind=kOutput, calls=%fused_computation.37 | convolution fusion | flops 3735552 | bytes 855552 | tf_op jit(solution)/shard_map/shed,shd->she/dot_general | solution.py:89
  56.5 2.1 %fusion.26 = f32[24,1,64]{2,1,0:T(1,128)S(1)} fusion(f32[24]{0:T(128)S(1)} %get-tuple-element.39, f32[24,128]{1,0:T(8,128)S(1)} %bitcast.329, f32[24,64]{1,0:T(8,128)S(1)} %subtract_multiply_fusion.5, f32[24]{0:T(128)S(1)} %get-tuple-element.38, f32[24,128]{1,0:T(8,128)S(1)} %bitcast.333, f32[24,64]{1,0:T(8,128)S(1)} %subtract_multiply_fusion.6, ...), kind=kOutput, calls=%fused_computation.35 | convolution fusion | flops 4325376 | bytes 880640 | tf_op jit(solution)/shard_map/shed,shd->she/dot_general | solution.py:89
  58.7 2.2 %multiply_add_fusion.3 = f32[24,1,64,128]{3,2,1,0:T(8,128)} fusion(f32[24,128]{1,0:T(8,128)S(1)} %bitcast.327, f32[24,64]{1,0:T(8,128)S(1)} %subtract_multiply_fusion.4, f32[24]{0:T(128)S(1)} %get-tuple-element.39, f32[24,128]{1,0:T(8,128)S(1)} %bitcast.330, f32[24,64]{1,0:T(8,128)S(1)} %subtract_multiply_fusion.5, f32[24]{0:T(128)S(1)} %get-tuple-element.38, ...), kind=kLoop, calls=%fused_computation.49 | loop fusion | flops 2359296 | bytes 1646976 | tf_op jit(solution)/shard_map/add | solution.py:91
  61.6 8.0 %all-to-all-done = bf16[16,1,24,4,128]{4,2,3,1,0:T(8,128)(2,1)S(1)} async-done(((bf16[16,1,24,4,128]{4,2,3,1,0:T(8,128)(2,1)}), bf16[16,1,24,4,128]{4,2,3,1,0:T(8,128)(2,1)S(1)}, u32[]{:S(2)}, u32[]{:S(2)}) %all-to-all-start) | async-done | bytes 393248 | tf_op jit(solution)/shard_map/all_to_all | solution.py:23
  69.8 4.4 %all_to_all.20 = bf16[2,16,24,4,128]{4,2,3,1,0:T(8,128)(2,1)S(1)} all-to-all(bf16[2,16,24,4,128]{4,2,3,1,0:T(8,128)(2,1)S(1)} %pad_maximum_fusion), channel_id=1, replica_groups=mesh['grp'=2,'dp'=8,'kv'=16,'tp'=2] {'tp'}, dimensions={0} | all-to-all | bytes 1572864 | tf_op jit(solution)/shard_map/all_to_all | solution.py:23
  77.3 1.7 %convolution_convert_fusion.3 = bf16[96,64]{0,1:T(8,128)(2,1)S(1)} fusion(bf16[1,64,4096]{2,1,0:T(8,128)(2,1)} %param.19, bf16[12,8,32,128]{3,2,1,0:T(8,128)(2,1)} %bitcast.309), kind=kOutput, calls=%fused_computation.10 | convolution fusion | flops 50337792 | bytes 1323008 | tf_op jit(solution)/shard_map/dot_general | solution.py:124
  79.3 2.1 %all_gather.9 = bf16[128,192]{1,0:T(8,128)(2,1)S(1)} all-gather(bf16[64,192]{1,0:T(8,128)(2,1)S(1)} %copy.103), channel_id=1, replica_groups=mesh['grp'=2,'dp'=8,'kv'=16,'tp'=2] {'tp'}, dimensions={0}, use_global_device_ids=true | all-gather | bytes 73728 | tf_op jit(solution)/shard_map/all_gather | solution.py:38
  81.4 1.7 %fusion.3 = f32[96,64]{0,1:T(8,128)S(1)} fusion(bf16[1,64,4096]{2,1,0:T(8,128)(2,1)} %param.22, bf16[12,8,32,128]{3,2,1,0:T(8,128)(2,1)} %bitcast.310), kind=kOutput, calls=%fused_computation.8 | convolution fusion | flops 50343936 | bytes 1335296 | tf_op jit(solution)/shard_map/dot_general | solution.py:124
  83.1 1.7 %fusion.4 = f32[96,64]{0,1:T(8,128)S(1)} fusion(bf16[1,64,4096]{2,1,0:T(8,128)(2,1)} %param.21, bf16[12,8,32,128]{3,2,1,0:T(8,128)(2,1)} %bitcast.311), kind=kOutput, calls=%fused_computation.12 | convolution fusion | flops 50343936 | bytes 1335296 | tf_op jit(solution)/shard_map/dot_general | solution.py:124
  90.1 1.4 fusion.24
  91.6 1.5 %fusion.22 = f32[24,1,64]{2,1,0:T(1,128)S(1)} fusion(f32[24,1,64,128]{3,2,1,0:T(8,128)S(1)} %copy-done.2, f32[24,128]{1,0:T(8,128)S(1)} %bitcast.336, f32[24,64]{1,0:T(8,128)S(1)} %subtract_multiply_fusion.3, f32[24]{0:T(128)S(1)} %get-tuple-element.9, f32[24,4,1,128]{3,1,0,2:T(4,128)S(1)} %multiply_multiply_fusion), kind=kOutput, calls=%fused_computation.31 | convolution fusion | flops 2949120 | bytes 829952 | tf_op jit(solution)/shard_map/shed,shd->she/dot_general | solution.py:174
  93.0 1.5 %fusion.20 = f32[24,1,64]{2,1,0:T(1,128)S(1)} fusion(f32[24,1,64,128]{3,2,1,0:T(8,128)S(1)} %copy-done.2, f32[24]{0:T(128)S(1)} %get-tuple-element.8, f32[24,128]{1,0:T(8,128)S(1)} %bitcast.337, f32[24,64]{1,0:T(8,128)S(1)} %subtract_multiply_fusion.3, f32[24]{0:T(128)S(1)} %get-tuple-element.9, f32[24,4,1,128]{3,1,0,2:T(4,128)S(1)} %broadcast_multiply_fusion), kind=kOutput, calls=%fused_computation.29 | convolution fusion | flops 3145728 | bytes 830464 | tf_op jit(solution)/shard_map/shed,shd->she/dot_general | solution.py:89
  94.6 2.0 %multiply_add_fusion.1 = f32[24,1,64,128]{3,2,1,0:T(8,128)S(1)} fusion(f32[24,128]{1,0:T(8,128)S(1)} %bitcast.348, f32[24,64]{1,0:T(8,128)S(1)} %subtract_multiply_fusion.2, f32[24]{0:T(128)S(1)} %get-tuple-element.8, f32[24,128]{1,0:T(8,128)S(1)} %bitcast.338, f32[24,64]{1,0:T(8,128)S(1)} %subtract_multiply_fusion.3, f32[24]{0:T(128)S(1)} %get-tuple-element.9, ...), kind=kLoop, calls=%fused_computation.47 | loop fusion | flops 3538944 | bytes 1684032 | tf_op jit(solution)/shard_map/add | solution.py:91
  98.0 1.4 fusion.16
  99.4 1.4 %fusion.14 = f32[24,1,64]{2,1,0:T(1,128)S(1)} fusion(f32[24,1,64,128]{3,2,1,0:T(8,128)S(1)} %multiply_add_fusion.1, f32[24,128]{1,0:T(8,128)S(1)} %bitcast.357, f32[24,64]{1,0:T(8,128)S(1)} %subtract_multiply_fusion.1, f32[24]{0:T(128)S(1)} %get-tuple-element.6, f32[24,4,1,128]{3,1,0,2:T(4,128)S(1)} %multiply_multiply_fusion), kind=kOutput, calls=%fused_computation.23 | convolution fusion | flops 2949120 | bytes 829952 | tf_op jit(solution)/shard_map/shed,shd->she/dot_general | solution.py:174
  100.9 1.5 %fusion.12 = f32[24,1,64]{2,1,0:T(1,128)S(1)} fusion(f32[24,1,64,128]{3,2,1,0:T(8,128)S(1)} %multiply_add_fusion.1, f32[24]{0:T(128)S(1)} %get-tuple-element.7, f32[24,128]{1,0:T(8,128)S(1)} %bitcast.358, f32[24,64]{1,0:T(8,128)S(1)} %subtract_multiply_fusion.1, f32[24]{0:T(128)S(1)} %get-tuple-element.6, f32[24,4,1,128]{3,1,0,2:T(4,128)S(1)} %broadcast_multiply_fusion), kind=kOutput, calls=%fused_computation.21 | convolution fusion | flops 3145728 | bytes 830464 | tf_op jit(solution)/shard_map/shed,shd->she/dot_general | solution.py:89
  102.4 1.7 %fusion.10 = f32[24,1,64]{2,1,0:T(1,128)S(1)} fusion(f32[24,1,64,128]{3,2,1,0:T(8,128)S(1)} %multiply_add_fusion.1, f32[24,128]{1,0:T(8,128)S(1)} %bitcast.366, f32[24,64]{1,0:T(8,128)S(1)} %subtract_multiply_fusion, f32[24]{0:T(128)S(1)} %get-tuple-element.7, f32[24,128]{1,0:T(8,128)S(1)} %bitcast.359, f32[24,64]{1,0:T(8,128)S(1)} %subtract_multiply_fusion.1, ...), kind=kOutput, calls=%fused_computation.19 | convolution fusion | flops 3538944 | bytes 855040 | tf_op jit(solution)/shard_map/shed,shd->she/dot_general | solution.py:174
  104.2 1.9 %all-gather.1 = f32[2,24,4]{1,2,0:T(4,128)S(1)} all-gather(f32[1,24,4]{1,2,0:T(4,128)S(1)} %bitcast.372), channel_id=2, replica_groups=mesh['grp'=2,'dp'=8,'kv'=16,'tp'=2] {'tp'}, dimensions={0}, use_global_device_ids=true | all-gather | bytes 1152 | tf_op jit(solution)/shard_map/all_gather | solution.py:47
  106.3 3.8 %all_to_all.21 = bf16[2,2,3072]{2,1,0:T(2,128)(2,1)S(1)} all-to-all(bf16[2,2,3072]{2,1,0:T(2,128)(2,1)S(1)} %reshape.857), channel_id=1, replica_groups=mesh['grp'=2,'dp'=8,'kv'=16,'tp'=2] {'tp'}, dimensions={0} | all-to-all | bytes 49152 | tf_op jit(solution)/shard_map/all_to_all | solution.py:53
  110.7 30.0 %all_to_all.22 = bf16[16,96,128]{2,1,0:T(8,128)(2,1)S(1)} all-to-all(bf16[16,96,128]{2,1,0:T(8,128)(2,1)S(1)} %bitcast.305), channel_id=1, replica_groups=mesh['grp'=2,'dp'=8,'kv'=16,'tp'=2] {'kv'}, dimensions={0} | all-to-all | bytes 786432 | tf_op jit(solution)/shard_map/all_to_all | solution.py:79
  (132 shorter events, 16.7 us)
Async XLA Ops:
  0.6 76.2 %copy-start = (bf16[1,64,4096]{2,1,0:T(8,128)(2,1)S(1)}, bf16[1,64,4096]{2,1,0:T(8,128)(2,1)}, u32[]{:S(2)}) copy-start(bf16[1,64,4096]{2,1,0:T(8,128)(2,1)} %param.20) | copy-start | bytes 1572868
  0.6 45.3 %copy-start.4 = (bf16[1,64,4096]{2,1,0:T(8,128)(2,1)S(1)}, bf16[1,64,4096]{2,1,0:T(8,128)(2,1)}, u32[]{:S(2)}) copy-start(bf16[1,64,4096]{2,1,0:T(8,128)(2,1)} %param.27) | copy-start | bytes 1572868
  2.3 67.4 %all-to-all-start = ((bf16[16,1,24,4,128]{4,2,3,1,0:T(8,128)(2,1)}), bf16[16,1,24,4,128]{4,2,3,1,0:T(8,128)(2,1)S(1)}, u32[]{:S(2)}, u32[]{:S(2)}) async-start(bf16[16,1,24,4,128]{4,2,3,1,0:T(8,128)(2,1)} %stack.31), calls=%async_computation | async-start | bytes 786432 | tf_op jit(solution)/shard_map/all_to_all | solution.py:23
  46.3 4.2 %copy-start.13 = (bf16[24,4,1,128]{3,1,2,0:T(4,128)(2,1)S(1)}, bf16[24,4,1,128]{3,1,2,0:T(4,128)(2,1)}, u32[]{:S(2)}) copy-start(bf16[24,4,1,128]{3,1,2,0:T(4,128)(2,1)} %param.29) | copy-start | bytes 73732
  46.4 4.4 %copy-start.12 = (bf16[24,4,1,64]{3,1,2,0:T(4,128)(2,1)S(1)}, bf16[24,4,1,64]{3,1,2,0:T(4,128)(2,1)}, u32[]{:S(2)}) copy-start(bf16[24,4,1,64]{3,1,2,0:T(4,128)(2,1)} %param.30) | copy-start | bytes 36868
  46.4 4.5 %copy-start.24 = (f32[24,4,1]{0,2,1:T(1,128)S(1)}, f32[24,4,1]{0,2,1:T(1,128)}, u32[]{:S(2)}) copy-start(f32[24,4,1]{0,2,1:T(1,128)} %param.32) | copy-start | bytes 1156
  46.4 4.5 %copy-start.25 = (f32[24,4,1]{0,2,1:T(1,128)S(1)}, f32[24,4,1]{0,2,1:T(1,128)}, u32[]{:S(2)}) copy-start(f32[24,4,1]{0,2,1:T(1,128)} %param.31) | copy-start | bytes 1156
  46.4 4.5 %copy-start.28 = (s32[24]{0:T(128)S(1)}, s32[24]{0:T(128)}, u32[]{:S(2)}) copy-start(s32[24]{0:T(128)} %param.33) | copy-start | bytes 292
  46.4 4.5 %copy-start.1 = (f32[24,1,64,128]{3,2,1,0:T(8,128)S(1)}, f32[24,1,64,128]{3,2,1,0:T(8,128)}, u32[]{:S(2)}) copy-start(f32[24,1,64,128]{3,2,1,0:T(8,128)} %param.28) | copy-start | bytes 2359300
  48.6 12.3 %collective-permute-start = (bf16[1,64,16,128]{3,2,1,0:T(8,128)(2,1)S(1)}, bf16[1,64,16,128]{3,2,1,0:T(8,128)(2,1)S(1)}, u32[]{:S(2)}, u32[]{:S(2)}) collective-permute-start(bf16[1,64,16,128]{3,2,1,0:T(8,128)(2,1)S(1)} %bitcast.316), channel_id=1, source_target_pairs={{0,1},{1,0},{2,3},{3,2},{4,5},{5,4},{6,7},{7,6},{8,9},{9,8},{10,11... | collective-permute-start | bytes 786440 | tf_op jit(solution)/shard_map/ppermute | solution.py:68
  50.9 7.7 %copy-start.20 = (f32[24]{0:T(128)}, f32[24]{0:T(128)S(1)}, u32[]{:S(2)}) copy-start(f32[24]{0:T(128)S(1)} %get-tuple-element.39) | copy-start | bytes 292
  50.9 7.7 %copy-start.22 = (f32[24]{0:T(128)}, f32[24]{0:T(128)S(1)}, u32[]{:S(2)}) copy-start(f32[24]{0:T(128)S(1)} %get-tuple-element.40) | copy-start | bytes 292
  56.4 4.4 %copy-start.8 = (f32[24,64]{1,0:T(8,128)}, f32[24,64]{1,0:T(8,128)S(1)}, u32[]{:S(2)}) copy-start(f32[24,64]{1,0:T(8,128)S(1)} %subtract_multiply_fusion.5) | copy-start | bytes 18436
  58.6 11.1 %copy-start.10 = (f32[24,64]{1,0:T(8,128)}, f32[24,64]{1,0:T(8,128)S(1)}, u32[]{:S(2)}) copy-start(f32[24,64]{1,0:T(8,128)S(1)} %subtract_multiply_fusion.4) | copy-start | bytes 18436
  88.7 2.8 %copy-start.19 = (f32[24,1,1,64]{3,1,0,2:T(1,128)S(1)}, f32[24,1,1,64]{3,1,0,2:T(1,128)}, u32[]{:S(2)}) copy-start(f32[24,1,1,64]{3,1,0,2:T(1,128)} %get-tuple-element.17) | copy-start | bytes 18436
  89.3 5.2 %copy-start.18 = (f32[24,1,1,64]{3,1,0,2:T(1,128)S(1)}, f32[24,1,1,64]{3,1,0,2:T(1,128)}, u32[]{:S(2)}) copy-start(f32[24,1,1,64]{3,1,0,2:T(1,128)} %get-tuple-element.16) | copy-start | bytes 18436
  89.3 5.2 %copy-start.9 = (f32[24,64]{1,0:T(8,128)S(1)}, f32[24,64]{1,0:T(8,128)}, u32[]{:S(2)}) copy-start(f32[24,64]{1,0:T(8,128)} %copy-done.8) | copy-start | bytes 18436
  89.3 5.2 %copy-start.11 = (f32[24,64]{1,0:T(8,128)S(1)}, f32[24,64]{1,0:T(8,128)}, u32[]{:S(2)}) copy-start(f32[24,64]{1,0:T(8,128)} %copy-done.10) | copy-start | bytes 18436
  89.4 5.2 %copy-start.21 = (f32[24]{0:T(128)S(1)}, f32[24]{0:T(128)}, u32[]{:S(2)}) copy-start(f32[24]{0:T(128)} %copy-done.20) | copy-start | bytes 292
  89.4 5.2 %copy-start.23 = (f32[24]{0:T(128)S(1)}, f32[24]{0:T(128)}, u32[]{:S(2)}) copy-start(f32[24]{0:T(128)} %copy-done.22) | copy-start | bytes 292
  94.6 4.7 %copy-start.17 = (f32[24,1,1,64]{3,1,0,2:T(1,128)S(1)}, f32[24,1,1,64]{3,1,0,2:T(1,128)}, u32[]{:S(2)}) copy-start(f32[24,1,1,64]{3,1,0,2:T(1,128)} %get-tuple-element.14) | copy-start | bytes 18436
  98.0 4.4 %copy-start.16 = (f32[24,1,1,64]{3,1,0,2:T(1,128)S(1)}, f32[24,1,1,64]{3,1,0,2:T(1,128)}, u32[]{:S(2)}) copy-start(f32[24,1,1,64]{3,1,0,2:T(1,128)} %get-tuple-element.15) | copy-start | bytes 18436
  100.9 5.2 %copy-start.27 = (f32[64]{0:T(128)S(1)}, f32[64]{0:T(128)}, u32[]{:S(2)}) copy-start(f32[64]{0:T(128)} %param.26) | copy-start | bytes 772
  100.9 9.5 %copy-start.5 = (bf16[8,8,16,128]{3,1,2,0:T(8,128)(2,1)S(1)}, bf16[8,8,16,128]{3,1,2,0:T(8,128)(2,1)}, u32[]{:S(2)}) copy-start(bf16[8,8,16,128]{3,1,2,0:T(8,128)(2,1)} %copy.177) | copy-start | bytes 786436
  (7 other events, 8.3 us)
